TPU v7x, 512 devices: a 4x2x32 block of a 4x8x32 slice. The times are simulated.
512 devices in a mesh: grp: 2 (over y), sp: 64 (over z, core), tp: 4 (over x).
Axes of the slice: x: 4, y: 2, z: 32, core: 2. Of those that a mesh axis runs over, the one named last changes fastest.
The devices are a block of a 4x8x32 slice.
Arguments:
- tokens: bfloat16 [131072, 2048], P(('grp', 'sp', 'tp')), parts along dimension 0, may hold values from -6 to 6
- step: float32 [131072], P(('grp', 'sp')), parts along dimension 0, may hold values from 0.2 to 3.75
- in_gain: float32 [2048], replicated, may hold values from 0.1 to 1.9
- in_proj: bfloat16 [2048, 512], P(None, 'tp'), may hold values from -0.125 to 0.125
- decay_rate: float32 [32, 64], P('tp'), may hold values from 1.5258789e-06 to 0.04
- frequency: float32 [32, 64], P('tp'), may hold values from 0.2 to 3
- input_map: float32 [2, 32, 64, 16], P(None, 'tp'), may hold values from -1 to 1
- readout: float32 [2, 32, 16, 64], P(None, 'tp'), may hold values from -0.75 to 0.75
- out_gain: float32 [512], replicated, may hold values from 0.1 to 1.9
- out_proj: bfloat16 [512, 2048], replicated, may hold values from -0.25 to 0.25
Outputs:
- mixed: bfloat16 [131072, 2048], P(('grp', 'sp', 'tp')), parts along dimension 0
There are 2 independent parts, one for each index of `grp`. A program takes and returns all parts, laid end to end along the dimension named above; an argument that names none is the same for every part. Nothing has to cross between parts.
All inputs are finite; a program needn't handle non-finite values.
Results may differ from a plain program's by a relative error of at most 0.01.
Values may be sent and summed in bfloat16 or wider, within the bound.
No kernel may reach another device: no remote copies, remote signals or barrier semaphores. Data moves between devices by JAX's collectives and lax.ppermute only.
A program may use at most 64 MiB of HBM per device.

v0:
```python
from functools import partial
import jax
import jax.numpy as jnp
from jax import lax
from jax.sharding import PartitionSpec as P

SPAN = 64
HIGHEST = lax.Precision.HIGHEST


def gathered_once(array, axis):
    leaves = jax.tree.leaves(array)
    sequence = sorted(range(len(leaves)), key=lambda k: -leaves[k].size)
    width = (1, *leaves[sequence[0]].shape)[-1]
    lines = [
        jnp.pad(leaves[k].reshape(-1), (0, -leaves[k].size % width)).reshape(-1, width)
        for k in sequence
    ]
    both, at, found = (lax.all_gather(jnp.concatenate(lines), axis), 0, {})
    for k, line in zip(sequence, lines):
        section = both[:, at : at + len(line)].reshape(len(both), -1)
        found[k] = section[:, : leaves[k].size].reshape(-1, *leaves[k].shape)
        at += len(line)
    numbers = iter(range(len(leaves)))
    return jax.tree.map(lambda _: found[next(numbers)], array)


def entering(value, axis, join, neutral):
    count, mine = (lax.axis_size(axis), lax.axis_index(axis))
    pieces = gathered_once(value, axis)
    so_far = jax.tree.map(
        lambda part, zero: jnp.full_like(part, 0) + jnp.asarray(zero, part.dtype), value, neutral
    )

    def lap(position, so_far):
        longer = join(so_far, jax.tree.map(lambda part: part[position], pieces))
        return jax.tree.map(lambda new, old: jnp.where(position < mine, new, old), longer, so_far)

    return lax.fori_loop(0, count - 1, lap, so_far)


def compose(earlier, later):
    a_re, a_im, b_re, b_im = earlier
    c_re, c_im, d_re, d_im = later
    return (
        c_re * a_re - c_im * a_im,
        c_re * a_im + c_im * a_re,
        c_re * b_re - c_im * b_im + d_re,
        c_re * b_im + c_im * b_re + d_im,
    )


def rms_rows(values, gain):
    values = values.astype(jnp.float32)
    scaled = values * lax.rsqrt(jnp.mean(values * values, axis=-1, keepdims=True) + 1e-06)
    return (scaled * gain).astype(jnp.bfloat16)


def block_tables(input_map, readout):
    groups = input_map.shape[1]
    unit = jnp.eye(groups, dtype=jnp.float32)
    push_re = jnp.einsum("gph,gk->ghkp", input_map[0], unit, precision=HIGHEST)
    push_im = jnp.einsum("gph,gk->ghkp", input_map[1], unit, precision=HIGHEST)
    read_re = jnp.einsum("ghp,gk->gpkh", readout[0], unit, precision=HIGHEST)
    read_im = jnp.einsum("ghp,gk->gpkh", readout[1], unit, precision=HIGHEST)
    inner = push_re.shape[0] * push_re.shape[1]
    flat = push_re.shape[2] * push_re.shape[3]
    return (
        push_re.reshape(inner, flat),
        push_im.reshape(inner, flat),
        read_re.reshape(flat, inner),
        read_im.reshape(flat, inner),
    )


def response(s_re, s_im, read_re, read_im):
    value = jnp.dot(s_re, read_re, precision=HIGHEST) - jnp.dot(s_im, read_im, precision=HIGHEST)
    return jax.nn.gelu(value, approximate=True).astype(jnp.bfloat16)


def advance(carry, piece, rates, freqs, tables, lower, keep):
    drive_part, time_part = piece
    push_re, push_im, read_re, read_im = tables
    own = time_part[:, None]
    magnitude = jnp.exp(-rates[None] * own)
    a_re = magnitude * jnp.cos(freqs[None] * own)
    a_im = magnitude * jnp.sin(freqs[None] * own)
    lam_re = -rates
    denom = lam_re * lam_re + freqs * freqs
    n_re = a_re - 1.0
    z_re = (n_re * lam_re + a_im * freqs) / denom
    z_im = (a_im * lam_re - n_re * freqs) / denom
    grouped = drive_part.astype(jnp.float32)
    in_re = jnp.dot(grouped, push_re, precision=HIGHEST)
    in_im = jnp.dot(grouped, push_im, precision=HIGHEST)
    i_re = z_re * in_re - z_im * in_im
    i_im = z_re * in_im + z_im * in_re
    elapsed = jnp.dot(lower, time_part, precision=HIGHEST)[:, None]
    grow = jnp.exp(rates[None] * elapsed)
    angle = freqs[None] * elapsed
    cosine = jnp.cos(angle)
    sine = jnp.sin(angle)
    w_re = grow * (cosine * i_re + sine * i_im)
    w_im = grow * (cosine * i_im - sine * i_re)
    acc_re = jnp.dot(lower, w_re, precision=HIGHEST)
    acc_im = jnp.dot(lower, w_im, precision=HIGHEST)
    shrink = jnp.exp(-rates[None] * elapsed)
    c_re = shrink * cosine
    c_im = shrink * sine
    s_re = c_re * acc_re - c_im * acc_im
    s_im = c_re * acc_im + c_im * acc_re
    d_re, d_im, e_re, e_im = carry
    full_re = s_re + c_re * e_re - c_im * e_im
    full_im = s_im + c_re * e_im + c_im * e_re
    cum_re = c_re * d_re - c_im * d_im
    cum_im = c_re * d_im + c_im * d_re
    ends = (cum_re[-1], cum_im[-1], full_re[-1], full_im[-1])
    return (ends, (cum_re, cum_im, full_re, full_im))


def on_device(
    tokens, step, in_gain, in_proj, decay_rate, frequency, input_map, readout, out_gain, out_proj
):
    normed = rms_rows(tokens, in_gain)
    rates, freqs, maps, reads = (decay_rate, frequency, input_map, readout)
    drive = jnp.dot(
        lax.all_gather(normed, "tp", axis=0, tiled=True),
        in_proj,
        preferred_element_type=jnp.float32,
    ).astype(jnp.bfloat16)
    tables = block_tables(maps, reads)
    flat_rates = rates.reshape(-1)
    flat_freqs = freqs.reshape(-1)
    seq_rows = drive.shape[0]
    block_count = seq_rows // SPAN
    drive_blocks = drive.reshape(block_count, SPAN, -1)
    time_blocks = step.reshape(block_count, SPAN)
    rows_index = lax.broadcasted_iota(jnp.int32, (SPAN, SPAN), 0)
    cols_index = lax.broadcasted_iota(jnp.int32, (SPAN, SPAN), 1)
    lower = (cols_index <= rows_index).astype(jnp.float32)
    zeros = jnp.zeros(flat_rates.shape, jnp.float32)
    ones = jnp.ones(flat_rates.shape, jnp.float32)
    start_carry = (ones, zeros, zeros, zeros)
    keep_first = "states"
    ends, stored = lax.scan(
        partial(
            advance, rates=flat_rates, freqs=flat_freqs, tables=tables, lower=lower, keep=keep_first
        ),
        start_carry,
        (drive_blocks, time_blocks),
    )
    incoming = entering(ends, "sp", compose, start_carry)
    cum_re, cum_im, full_re, full_im = stored
    width = flat_rates.shape[0]
    cum_re = cum_re.reshape(seq_rows, width)
    cum_im = cum_im.reshape(seq_rows, width)
    state_re = full_re.reshape(seq_rows, width) + cum_re * incoming[2] - cum_im * incoming[3]
    state_im = full_im.reshape(seq_rows, width) + cum_re * incoming[3] + cum_im * incoming[2]
    answer = response(state_re, state_im, tables[2], tables[3])
    gathered = lax.all_to_all(answer, "tp", split_axis=0, concat_axis=1, tiled=True)
    shaped = rms_rows(gathered, out_gain)
    return jnp.dot(shaped, out_proj, preferred_element_type=jnp.float32).astype(jnp.bfloat16)


def solution(mesh):
    placed = (
        P(("grp", "sp", "tp"), None),
        P(("grp", "sp")),
        P(),
        P(None, "tp"),
        P("tp", None),
        P("tp", None),
        P(None, "tp", None, None),
        P(None, "tp", None, None),
        P(),
        P(),
    )
    return jax.shard_map(
        on_device,
        mesh=mesh,
        in_specs=placed,
        out_specs=P(("grp", "sp", "tp"), None),
        check_vma=False,
    )
```

profile of v0, /device:TPU:33, one launch (start us, length us, event | category | flops | bytes accessed | tf_op | source)
XLA Modules:
  0.0 373.2 jit_solution(620879934638658215)
XLA Ops:
  6.6 1.7 fusion.44
  8.3 2.5 fusion.46
  15.7 85.1 %all-gather.4.cloned.1.call-done = bf16[1024,2048]{1,0:T(8,128)(2,1)} async-done(((bf16[256,2048]{1,0:T(8,128)(2,1)}), bf16[1024,2048]{1,0:T(8,128)(2,1)}) %all-gather.4.cloned.1.call-update) | async-done | bytes 4194320 | tf_op jit(solution)/shard_map/all_gather | solution.py:127
  100.8 4.3 %convolution_convert_fusion.1 = bf16[1024,128]{1,0:T(8,128)(2,1)} fusion(bf16[1024,2048]{1,0:T(8,128)(2,1)} %all-gather.4.cloned.1.call-done, bf16[2048,128]{1,0:T(8,128)(2,1)} %param.17), kind=kOutput, calls=%fused_computation.81 | convolution fusion | flops 537001984 | bytes 4980736 | tf_op jit(solution)/shard_map/dot_general | solution.py:126
  106.2 173.9 %while.48 = (s32[]{:T(128)}, f32[512]{0:T(512)S(1)}, f32[512]{0:T(512)S(1)}, f32[512]{0:T(512)}, f32[512]{0:T(512)}, /*index=5*/f32[16,64,512]{2,1,0:T(8,128)}, ...) while((s32[]{:T(128)}, f32[512]{0:T(512)S(1)}, ...), condition=%wide.wide.region_2.3_spmd.clone.clone.clone, body=%wide.wide.region_1.2_spmd.clone.clone.clone.sunk | while | flops 153889792 | bytes 4405837 | solution.py:145
  106.6 1.0 fusion.103
  110.2 2.0 convolution_bitcast_fusion.8
  112.3 3.0 add_dynamic-update-slice_fusion.3
  117.4 1.0 fusion.103
  118.5 1.0 fusion.104
  121.1 2.0 convolution_bitcast_fusion.8
  123.2 3.0 add_dynamic-update-slice_fusion.3
  128.3 1.0 fusion.103
  129.4 1.0 fusion.104
  131.9 2.0 convolution_bitcast_fusion.8
  134.1 3.0 add_dynamic-update-slice_fusion.3
  139.2 1.0 fusion.103
  140.3 1.0 fusion.104
  142.8 2.0 convolution_bitcast_fusion.8
  144.9 3.0 add_dynamic-update-slice_fusion.3
  150.1 1.0 fusion.103
  151.2 1.0 fusion.104
  153.7 2.0 convolution_bitcast_fusion.8
  155.8 3.0 add_dynamic-update-slice_fusion.3
  160.9 1.0 fusion.103
  162.1 1.0 fusion.104
  164.6 2.0 convolution_bitcast_fusion.8
  166.7 3.0 add_dynamic-update-slice_fusion.3
  171.8 1.0 fusion.103
  172.9 1.0 fusion.104
  175.5 2.0 convolution_bitcast_fusion.8
  177.6 3.0 add_dynamic-update-slice_fusion.3
  182.7 1.0 fusion.103
  183.8 1.0 fusion.104
  186.3 2.0 convolution_bitcast_fusion.8
  188.4 3.0 add_dynamic-update-slice_fusion.3
  193.6 1.0 fusion.103
  194.7 1.0 fusion.104
  197.2 2.0 convolution_bitcast_fusion.8
  199.3 3.0 add_dynamic-update-slice_fusion.3
  208.1 2.0 convolution_bitcast_fusion.8
  210.2 3.0 add_dynamic-update-slice_fusion.3
  218.9 2.0 convolution_bitcast_fusion.8
  221.0 3.0 add_dynamic-update-slice_fusion.3
  226.1 1.0 fusion.103
  229.8 2.0 convolution_bitcast_fusion.8
  231.9 3.0 add_dynamic-update-slice_fusion.3
  238.1 1.0 fusion.104
  240.7 2.0 convolution_bitcast_fusion.8
  242.8 3.0 add_dynamic-update-slice_fusion.3
  251.5 2.0 convolution_bitcast_fusion.8
  253.6 3.0 add_dynamic-update-slice_fusion.3
  258.8 1.0 fusion.103
  262.4 2.0 convolution_bitcast_fusion.8
  264.5 3.0 add_dynamic-update-slice_fusion.3
  273.3 2.0 convolution_bitcast_fusion.8
  275.4 3.0 add_dynamic-update-slice_fusion.3
  280.9 60.4 %all-gather.1 = f32[64,4,512]{2,1,0:T(4,128)S(1)} all-gather(f32[1,4,512]{2,1,0:T(4,128)S(1)} %maximum_bitcast_fusion), channel_id=2, replica_groups=mesh['grp'=2,'sp'=64,'tp'=4] {'sp'}, dimensions={0}, use_global_device_ids=true | all-gather | bytes 532480 | tf_op jit(solution)/shard_map/all_gather | solution.py:19
  341.7 5.1 %while.47 = (s32[]{:T(128)}, f32[512]{0:T(512)S(1)}, f32[512]{0:T(512)S(1)}, s32[]{:T(128)}, f32[64,512]{1,0:T(8,128)S(1)}, /*index=5*/f32[64,512]{1,0:T(8,128)S...) while((s32[]{:T(128)}, f32[512]{0:T(512)S(1)}, f32[512]{0:T(512)S(1)}, ...), condition=%wide.region_4.5_spmd.clone, body=%wide.region_3.4_spmd.clone.sunk | while | flops 6148 | bytes 32897 | solution.py:39
  346.8 4.6 %multiply_add_fusion.5 = (f32[16,64,512]{2,1,0:T(8,128)S(1)}, f32[16,64,512]{2,1,0:T(8,128)S(1)}) fusion(f32[16,64,512]{2,1,0:T(8,128)} %get-tuple-element.435, f32[16,64,512]{2,1,0:T(8,128)} %get-tuple-element.437, f32[16,64,512]{2,1,0:T(8,128)} %get-tuple-element.429, f32[512]{0:T(512)S(1)} %get-tuple-element.436, f32[512]{0:T(512)S(1)} %get-tuple-element.434, ...), kind=kLoop, calls=%fused_computation.78 | loop fusion | flops 4194304 | bytes 12587008 | tf_op jit(solution)/shard_map/add | solution.py:158
  351.4 1.8 fusion.59
  353.3 1.8 fusion.54
  355.2 9.2 %all_to_all.13 = bf16[4,256,128]{1,2,0:T(8,128)(2,1)S(1)} all-to-all(bf16[4,256,128]{1,2,0:T(8,128)(2,1)S(1)} %copy.20), channel_id=1, replica_groups=mesh['grp'=2,'sp'=64,'tp'=4] {'tp'}, dimensions={0} | all-to-all | bytes 524288 | tf_op jit(solution)/shard_map/all_to_all | solution.py:160
  364.7 1.7 convolution_convert_fusion
  (595 shorter events, 81.8 us)
Async XLA Ops:
  6.5 358.1 %copy-start = (bf16[512,2048]{1,0:T(8,128)(2,1)S(1)}, bf16[512,2048]{1,0:T(8,128)(2,1)}, u32[]{:S(2)}) copy-start(bf16[512,2048]{1,0:T(8,128)(2,1)} %param.23) | copy-start | bytes 6291460
  6.6 6.4 %copy-start.12 = (f32[1024]{0:T(1024)S(1)}, f32[1024]{0:T(1024)}, u32[]{:S(2)}) copy-start(f32[1024]{0:T(1024)} %param.15) | copy-start | bytes 12292
  6.6 7.0 %copy-start.3 = (f32[2,8,16,64]{3,2,1,0:T(8,128)S(1)}, f32[2,8,16,64]{3,2,1,0:T(8,128)}, u32[]{:S(2)}) copy-start(f32[2,8,16,64]{3,2,1,0:T(8,128)} %param.21) | copy-start | bytes 196612
  6.6 94.2 %all-gather.4.cloned.1.call-start = ((), (), s32[]{:S(2)}) async-start(), calls=%async_computation.1 | async-start | bytes 5242880 | tf_op jit(solution)/shard_map/all_gather | solution.py:127
  106.5 5.7 %copy-start.5 = (f32[1,512]{1,0:T(1,128)S(1)}, f32[1,512]{1,0:T(1,128)}, u32[]{:S(2)}) copy-start(f32[1,512]{1,0:T(1,128)} %get-tuple-element.1028) | copy-start | bytes 6148 | tf_op jit(solution)/shard_map/while
  106.5 5.7 %copy-start.10 = (f32[512]{0:T(512)S(1)}, f32[512]{0:T(512)}, u32[]{:S(2)}) copy-start(f32[512]{0:T(512)} %get-tuple-element.1001) | copy-start | bytes 6148 | tf_op jit(solution)/shard_map/while
  106.5 5.7 %copy-start.11 = (f32[512]{0:T(512)S(1)}, f32[512]{0:T(512)}, u32[]{:S(2)}) copy-start(f32[512]{0:T(512)} %get-tuple-element.1002) | copy-start | bytes 6148 | tf_op jit(solution)/shard_map/while
  106.5 5.7 %copy-start.14 = (f32[512]{0:T(512)S(1)}, f32[512]{0:T(512)}, u32[]{:S(2)}) copy-start(f32[512]{0:T(512)} %get-tuple-element.1038) | copy-start | bytes 6148 | tf_op jit(solution)/shard_map/while
  106.6 5.7 %copy-start.15 = (f32[1,512]{1,0:T(1,128)S(1)}, f32[1,512]{1,0:T(1,128)}, u32[]{:S(2)}) copy-start(f32[1,512]{1,0:T(1,128)} %get-tuple-element.1032) | copy-start | bytes 6148 | tf_op jit(solution)/shard_map/while
  117.4 5.7 %copy-start.5 = (f32[1,512]{1,0:T(1,128)S(1)}, f32[1,512]{1,0:T(1,128)}, u32[]{:S(2)}) copy-start(f32[1,512]{1,0:T(1,128)} %get-tuple-element.1028) | copy-start | bytes 6148 | tf_op jit(solution)/shard_map/while
  117.4 5.7 %copy-start.10 = (f32[512]{0:T(512)S(1)}, f32[512]{0:T(512)}, u32[]{:S(2)}) copy-start(f32[512]{0:T(512)} %get-tuple-element.1001) | copy-start | bytes 6148 | tf_op jit(solution)/shard_map/while
  128.3 5.7 %copy-start.5 = (f32[1,512]{1,0:T(1,128)S(1)}, f32[1,512]{1,0:T(1,128)}, u32[]{:S(2)}) copy-start(f32[1,512]{1,0:T(1,128)} %get-tuple-element.1028) | copy-start | bytes 6148 | tf_op jit(solution)/shard_map/while
  128.3 5.7 %copy-start.10 = (f32[512]{0:T(512)S(1)}, f32[512]{0:T(512)}, u32[]{:S(2)}) copy-start(f32[512]{0:T(512)} %get-tuple-element.1001) | copy-start | bytes 6148 | tf_op jit(solution)/shard_map/while
  128.3 5.7 %copy-start.11 = (f32[512]{0:T(512)S(1)}, f32[512]{0:T(512)}, u32[]{:S(2)}) copy-start(f32[512]{0:T(512)} %get-tuple-element.1002) | copy-start | bytes 6148 | tf_op jit(solution)/shard_map/while
  128.3 5.7 %copy-start.14 = (f32[512]{0:T(512)S(1)}, f32[512]{0:T(512)}, u32[]{:S(2)}) copy-start(f32[512]{0:T(512)} %get-tuple-element.1038) | copy-start | bytes 6148 | tf_op jit(solution)/shard_map/while
  128.3 5.7 %copy-start.15 = (f32[1,512]{1,0:T(1,128)S(1)}, f32[1,512]{1,0:T(1,128)}, u32[]{:S(2)}) copy-start(f32[1,512]{1,0:T(1,128)} %get-tuple-element.1032) | copy-start | bytes 6148 | tf_op jit(solution)/shard_map/while
  139.1 5.7 %copy-start.5 = (f32[1,512]{1,0:T(1,128)S(1)}, f32[1,512]{1,0:T(1,128)}, u32[]{:S(2)}) copy-start(f32[1,512]{1,0:T(1,128)} %get-tuple-element.1028) | copy-start | bytes 6148 | tf_op jit(solution)/shard_map/while
  139.2 5.7 %copy-start.10 = (f32[512]{0:T(512)S(1)}, f32[512]{0:T(512)}, u32[]{:S(2)}) copy-start(f32[512]{0:T(512)} %get-tuple-element.1001) | copy-start | bytes 6148 | tf_op jit(solution)/shard_map/while
  139.2 5.7 %copy-start.11 = (f32[512]{0:T(512)S(1)}, f32[512]{0:T(512)}, u32[]{:S(2)}) copy-start(f32[512]{0:T(512)} %get-tuple-element.1002) | copy-start | bytes 6148 | tf_op jit(solution)/shard_map/while
  139.2 5.7 %copy-start.14 = (f32[512]{0:T(512)S(1)}, f32[512]{0:T(512)}, u32[]{:S(2)}) copy-start(f32[512]{0:T(512)} %get-tuple-element.1038) | copy-start | bytes 6148 | tf_op jit(solution)/shard_map/while
  139.2 5.7 %copy-start.15 = (f32[1,512]{1,0:T(1,128)S(1)}, f32[1,512]{1,0:T(1,128)}, u32[]{:S(2)}) copy-start(f32[1,512]{1,0:T(1,128)} %get-tuple-element.1032) | copy-start | bytes 6148 | tf_op jit(solution)/shard_map/while
  150.0 5.7 %copy-start.5 = (f32[1,512]{1,0:T(1,128)S(1)}, f32[1,512]{1,0:T(1,128)}, u32[]{:S(2)}) copy-start(f32[1,512]{1,0:T(1,128)} %get-tuple-element.1028) | copy-start | bytes 6148 | tf_op jit(solution)/shard_map/while
  150.0 5.7 %copy-start.10 = (f32[512]{0:T(512)S(1)}, f32[512]{0:T(512)}, u32[]{:S(2)}) copy-start(f32[512]{0:T(512)} %get-tuple-element.1001) | copy-start | bytes 6148 | tf_op jit(solution)/shard_map/while
  150.0 5.7 %copy-start.11 = (f32[512]{0:T(512)S(1)}, f32[512]{0:T(512)}, u32[]{:S(2)}) copy-start(f32[512]{0:T(512)} %get-tuple-element.1002) | copy-start | bytes 6148 | tf_op jit(solution)/shard_map/while
  150.0 5.7 %copy-start.14 = (f32[512]{0:T(512)S(1)}, f32[512]{0:T(512)}, u32[]{:S(2)}) copy-start(f32[512]{0:T(512)} %get-tuple-element.1038) | copy-start | bytes 6148 | tf_op jit(solution)/shard_map/while
  150.1 5.7 %copy-start.15 = (f32[1,512]{1,0:T(1,128)S(1)}, f32[1,512]{1,0:T(1,128)}, u32[]{:S(2)}) copy-start(f32[1,512]{1,0:T(1,128)} %get-tuple-element.1032) | copy-start | bytes 6148 | tf_op jit(solution)/shard_map/while
  160.9 5.7 %copy-start.5 = (f32[1,512]{1,0:T(1,128)S(1)}, f32[1,512]{1,0:T(1,128)}, u32[]{:S(2)}) copy-start(f32[1,512]{1,0:T(1,128)} %get-tuple-element.1028) | copy-start | bytes 6148 | tf_op jit(solution)/shard_map/while
  160.9 5.7 %copy-start.10 = (f32[512]{0:T(512)S(1)}, f32[512]{0:T(512)}, u32[]{:S(2)}) copy-start(f32[512]{0:T(512)} %get-tuple-element.1001) | copy-start | bytes 6148 | tf_op jit(solution)/shard_map/while
  160.9 5.7 %copy-start.11 = (f32[512]{0:T(512)S(1)}, f32[512]{0:T(512)}, u32[]{:S(2)}) copy-start(f32[512]{0:T(512)} %get-tuple-element.1002) | copy-start | bytes 6148 | tf_op jit(solution)/shard_map/while
  160.9 5.7 %copy-start.14 = (f32[512]{0:T(512)S(1)}, f32[512]{0:T(512)}, u32[]{:S(2)}) copy-start(f32[512]{0:T(512)} %get-tuple-element.1038) | copy-start | bytes 6148 | tf_op jit(solution)/shard_map/while
  160.9 5.7 %copy-start.15 = (f32[1,512]{1,0:T(1,128)S(1)}, f32[1,512]{1,0:T(1,128)}, u32[]{:S(2)}) copy-start(f32[1,512]{1,0:T(1,128)} %get-tuple-element.1032) | copy-start | bytes 6148 | tf_op jit(solution)/shard_map/while
  171.8 5.7 %copy-start.5 = (f32[1,512]{1,0:T(1,128)S(1)}, f32[1,512]{1,0:T(1,128)}, u32[]{:S(2)}) copy-start(f32[1,512]{1,0:T(1,128)} %get-tuple-element.1028) | copy-start | bytes 6148 | tf_op jit(solution)/shard_map/while
  171.8 5.7 %copy-start.10 = (f32[512]{0:T(512)S(1)}, f32[512]{0:T(512)}, u32[]{:S(2)}) copy-start(f32[512]{0:T(512)} %get-tuple-element.1001) | copy-start | bytes 6148 | tf_op jit(solution)/shard_map/while
  171.8 5.7 %copy-start.11 = (f32[512]{0:T(512)S(1)}, f32[512]{0:T(512)}, u32[]{:S(2)}) copy-start(f32[512]{0:T(512)} %get-tuple-element.1002) | copy-start | bytes 6148 | tf_op jit(solution)/shard_map/while
  171.8 5.7 %copy-start.14 = (f32[512]{0:T(512)S(1)}, f32[512]{0:T(512)}, u32[]{:S(2)}) copy-start(f32[512]{0:T(512)} %get-tuple-element.1038) | copy-start | bytes 6148 | tf_op jit(solution)/shard_map/while
  171.8 5.7 %copy-start.15 = (f32[1,512]{1,0:T(1,128)S(1)}, f32[1,512]{1,0:T(1,128)}, u32[]{:S(2)}) copy-start(f32[1,512]{1,0:T(1,128)} %get-tuple-element.1032) | copy-start | bytes 6148 | tf_op jit(solution)/shard_map/while
  182.6 5.7 %copy-start.5 = (f32[1,512]{1,0:T(1,128)S(1)}, f32[1,512]{1,0:T(1,128)}, u32[]{:S(2)}) copy-start(f32[1,512]{1,0:T(1,128)} %get-tuple-element.1028) | copy-start | bytes 6148 | tf_op jit(solution)/shard_map/while
  182.6 5.7 %copy-start.10 = (f32[512]{0:T(512)S(1)}, f32[512]{0:T(512)}, u32[]{:S(2)}) copy-start(f32[512]{0:T(512)} %get-tuple-element.1001) | copy-start | bytes 6148 | tf_op jit(solution)/shard_map/while
  182.7 5.7 %copy-start.11 = (f32[512]{0:T(512)S(1)}, f32[512]{0:T(512)}, u32[]{:S(2)}) copy-start(f32[512]{0:T(512)} %get-tuple-element.1002) | copy-start | bytes 6148 | tf_op jit(solution)/shard_map/while
  182.7 5.7 %copy-start.14 = (f32[512]{0:T(512)S(1)}, f32[512]{0:T(512)}, u32[]{:S(2)}) copy-start(f32[512]{0:T(512)} %get-tuple-element.1038) | copy-start | bytes 6148 | tf_op jit(solution)/shard_map/while
  182.7 5.7 %copy-start.15 = (f32[1,512]{1,0:T(1,128)S(1)}, f32[1,512]{1,0:T(1,128)}, u32[]{:S(2)}) copy-start(f32[1,512]{1,0:T(1,128)} %get-tuple-element.1032) | copy-start | bytes 6148 | tf_op jit(solution)/shard_map/while
  193.5 5.7 %copy-start.5 = (f32[1,512]{1,0:T(1,128)S(1)}, f32[1,512]{1,0:T(1,128)}, u32[]{:S(2)}) copy-start(f32[1,512]{1,0:T(1,128)} %get-tuple-element.1028) | copy-start | bytes 6148 | tf_op jit(solution)/shard_map/while
  193.5 5.7 %copy-start.10 = (f32[512]{0:T(512)S(1)}, f32[512]{0:T(512)}, u32[]{:S(2)}) copy-start(f32[512]{0:T(512)} %get-tuple-element.1001) | copy-start | bytes 6148 | tf_op jit(solution)/shard_map/while
  193.5 5.7 %copy-start.11 = (f32[512]{0:T(512)S(1)}, f32[512]{0:T(512)}, u32[]{:S(2)}) copy-start(f32[512]{0:T(512)} %get-tuple-element.1002) | copy-start | bytes 6148 | tf_op jit(solution)/shard_map/while
  193.5 5.7 %copy-start.14 = (f32[512]{0:T(512)S(1)}, f32[512]{0:T(512)}, u32[]{:S(2)}) copy-start(f32[512]{0:T(512)} %get-tuple-element.1038) | copy-start | bytes 6148 | tf_op jit(solution)/shard_map/while
  193.5 5.7 %copy-start.15 = (f32[1,512]{1,0:T(1,128)S(1)}, f32[1,512]{1,0:T(1,128)}, u32[]{:S(2)}) copy-start(f32[1,512]{1,0:T(1,128)} %get-tuple-element.1032) | copy-start | bytes 6148 | tf_op jit(solution)/shard_map/while
  226.1 5.7 %copy-start.5 = (f32[1,512]{1,0:T(1,128)S(1)}, f32[1,512]{1,0:T(1,128)}, u32[]{:S(2)}) copy-start(f32[1,512]{1,0:T(1,128)} %get-tuple-element.1028) | copy-start | bytes 6148 | tf_op jit(solution)/shard_map/while
  226.1 5.7 %copy-start.10 = (f32[512]{0:T(512)S(1)}, f32[512]{0:T(512)}, u32[]{:S(2)}) copy-start(f32[512]{0:T(512)} %get-tuple-element.1001) | copy-start | bytes 6148 | tf_op jit(solution)/shard_map/while
  226.1 5.7 %copy-start.11 = (f32[512]{0:T(512)S(1)}, f32[512]{0:T(512)}, u32[]{:S(2)}) copy-start(f32[512]{0:T(512)} %get-tuple-element.1002) | copy-start | bytes 6148 | tf_op jit(solution)/shard_map/while
  226.1 5.7 %copy-start.14 = (f32[512]{0:T(512)S(1)}, f32[512]{0:T(512)}, u32[]{:S(2)}) copy-start(f32[512]{0:T(512)} %get-tuple-element.1038) | copy-start | bytes 6148 | tf_op jit(solution)/shard_map/while
  226.1 5.7 %copy-start.15 = (f32[1,512]{1,0:T(1,128)S(1)}, f32[1,512]{1,0:T(1,128)}, u32[]{:S(2)}) copy-start(f32[1,512]{1,0:T(1,128)} %get-tuple-element.1032) | copy-start | bytes 6148 | tf_op jit(solution)/shard_map/while
  237.0 5.7 %copy-start.5 = (f32[1,512]{1,0:T(1,128)S(1)}, f32[1,512]{1,0:T(1,128)}, u32[]{:S(2)}) copy-start(f32[1,512]{1,0:T(1,128)} %get-tuple-element.1028) | copy-start | bytes 6148 | tf_op jit(solution)/shard_map/while
  237.0 5.7 %copy-start.10 = (f32[512]{0:T(512)S(1)}, f32[512]{0:T(512)}, u32[]{:S(2)}) copy-start(f32[512]{0:T(512)} %get-tuple-element.1001) | copy-start | bytes 6148 | tf_op jit(solution)/shard_map/while
  237.0 5.7 %copy-start.11 = (f32[512]{0:T(512)S(1)}, f32[512]{0:T(512)}, u32[]{:S(2)}) copy-start(f32[512]{0:T(512)} %get-tuple-element.1002) | copy-start | bytes 6148 | tf_op jit(solution)/shard_map/while
  237.0 5.7 %copy-start.14 = (f32[512]{0:T(512)S(1)}, f32[512]{0:T(512)}, u32[]{:S(2)}) copy-start(f32[512]{0:T(512)} %get-tuple-element.1038) | copy-start | bytes 6148 | tf_op jit(solution)/shard_map/while
  237.0 5.7 %copy-start.15 = (f32[1,512]{1,0:T(1,128)S(1)}, f32[1,512]{1,0:T(1,128)}, u32[]{:S(2)}) copy-start(f32[1,512]{1,0:T(1,128)} %get-tuple-element.1032) | copy-start | bytes 6148 | tf_op jit(solution)/shard_map/while
  258.7 5.7 %copy-start.5 = (f32[1,512]{1,0:T(1,128)S(1)}, f32[1,512]{1,0:T(1,128)}, u32[]{:S(2)}) copy-start(f32[1,512]{1,0:T(1,128)} %get-tuple-element.1028) | copy-start | bytes 6148 | tf_op jit(solution)/shard_map/while
  258.7 5.7 %copy-start.10 = (f32[512]{0:T(512)S(1)}, f32[512]{0:T(512)}, u32[]{:S(2)}) copy-start(f32[512]{0:T(512)} %get-tuple-element.1001) | copy-start | bytes 6148 | tf_op jit(solution)/shard_map/while
  258.7 5.7 %copy-start.11 = (f32[512]{0:T(512)S(1)}, f32[512]{0:T(512)}, u32[]{:S(2)}) copy-start(f32[512]{0:T(512)} %get-tuple-element.1002) | copy-start | bytes 6148 | tf_op jit(solution)/shard_map/while
  258.7 5.7 %copy-start.14 = (f32[512]{0:T(512)S(1)}, f32[512]{0:T(512)}, u32[]{:S(2)}) copy-start(f32[512]{0:T(512)} %get-tuple-element.1038) | copy-start | bytes 6148 | tf_op jit(solution)/shard_map/while
  258.8 5.7 %copy-start.15 = (f32[1,512]{1,0:T(1,128)S(1)}, f32[1,512]{1,0:T(1,128)}, u32[]{:S(2)}) copy-start(f32[1,512]{1,0:T(1,128)} %get-tuple-element.1032) | copy-start | bytes 6148 | tf_op jit(solution)/shard_map/while
  280.2 61.5 %copy-start.6 = (f32[512]{0:T(512)S(1)}, f32[512]{0:T(512)}, u32[]{:S(2)}) copy-start(f32[512]{0:T(512)} %custom-call) | copy-start | bytes 6148
  280.2 61.5 %copy-start.7 = (f32[512]{0:T(512)S(1)}, f32[512]{0:T(512)}, u32[]{:S(2)}) copy-start(f32[512]{0:T(512)} %custom-call.1) | copy-start | bytes 6148
  353.2 11.3 %copy-start.13 = (f32[512]{0:T(512)S(1)}, f32[512]{0:T(512)}, u32[]{:S(2)}) copy-start(f32[512]{0:T(512)} %param.22) | copy-start | bytes 6148
  (28 other events, 152.0 us)
Sparse Core Ops, SparseCore 0:
  11.0 89.7 all-gather.3
where the time goes:
time: 378 us; the launch traced here: 373 us
  matrix products  134 us (35%)
  waiting for transfers between devices  85.1 us (23%)
  blocking collectives  69.5 us (18%)
  local copies, waits for them, and re-layouts  43.1 us (11%)
  other arithmetic  22.5 us (6%)
  between operations  13.7 us (4%)
  loops' own time  5.22 us (1%)
    all_gather x1, waiting for transfers between devices, on_device(): lax.all_gather(normed, 'tp', axis=0, tiled=True)  85.1 us
    all_gather x1, blocking collectives, gathered_once(): both, at, found = (lax.all_gather(jnp.concatenate(lines), axis), 0, {})  60.4 us
    dot_general x16, matrix products, advance(): acc_im = jnp.dot(lower, w_im, precision=HIGHEST)  48.1 us
    dot_general x16, matrix products, advance(): acc_re = jnp.dot(lower, w_re, precision=HIGHEST)  32.4 us
    slice x32, local copies, waits for them, and re-layouts, advance(): ends = (cum_re[-1], cum_im[-1], full_re[-1], full_im[-1])  18.8 us
    dot_general x16, matrix products, advance(): in_im = jnp.dot(grouped, push_im, precision=HIGHEST)  15.3 us
    dot_general x16, matrix products, advance(): in_re = jnp.dot(grouped, push_re, precision=HIGHEST)  15.3 us
    dot_general x16, matrix products, advance(): elapsed = jnp.dot(lower, time_part, precision=HIGHEST)[:, None]  13.3 us
  transfers between devices with their start and end apart: 1, of which 1 were waited for; matrix products, arithmetic and copies ran while one was open for 1% of the time, Pallas kernels for 0%

commit v1 on v0

--- a/solution.py
+++ b/solution.py
@@ -6,6 +6,11 @@
 
 SPAN = 64
 HIGHEST = lax.Precision.HIGHEST
+
+
+def gather_by_exchange(array, axis, dim):
+    copies = jnp.concatenate([array] * lax.axis_size(axis), axis=dim)
+    return lax.all_to_all(copies, axis, dim, dim, tiled=True)
 
 
 def gathered_once(array, axis):
@@ -124,9 +129,7 @@
     normed = rms_rows(tokens, in_gain)
     rates, freqs, maps, reads = (decay_rate, frequency, input_map, readout)
     drive = jnp.dot(
-        lax.all_gather(normed, "tp", axis=0, tiled=True),
-        in_proj,
-        preferred_element_type=jnp.float32,
+        gather_by_exchange(normed, "tp", 0), in_proj, preferred_element_type=jnp.float32
     ).astype(jnp.bfloat16)
     tables = block_tables(maps, reads)
     flat_rates = rates.reshape(-1)

time: 378 us -> 367 us (0.971)
  waiting for transfers between devices: 85.1 us -> 22.5 us
  blocking collectives: 69.5 us -> 129 us
  between operations: 13.7 us -> 0.25 us
  starting transfers between devices: 0.06 us -> 5.26 us
    all_gather x1 -> x0, waiting for transfers between devices: 85.1 us -> none  [on_device(): lax.all_gather(normed, 'tp', axis=0, tiled=True)]
    all_gather x1, blocking collectives: 60.4 us -> 120 us  [gathered_once(): both, at, found = (lax.all_gather(jnp.concatenate(lines), axis), 0, {})]
    all_to_all x0 -> x1, waiting for transfers between devices: none -> 22.5 us  [gather_by_exchange(): return lax.all_to_all(copies, axis, dim, dim, tiled=True)]
    all_to_all x0 -> x1, starting transfers between devices: none -> 5.26 us  [gather_by_exchange(): return lax.all_to_all(copies, axis, dim, dim, tiled=True)]
where the time goes in v1:
time: 367 us; the launch traced here: 362 us
  matrix products  134 us (37%)
  blocking collectives  129 us (35%)
  local copies, waits for them, and re-layouts  42.6 us (12%)
  other arithmetic  23.8 us (6%)
  waiting for transfers between devices  22.5 us (6%)
  starting transfers between devices  5.26 us (1%)
  loops' own time  5.22 us (1%)
    all_gather x1, blocking collectives, gathered_once(): both, at, found = (lax.all_gather(jnp.concatenate(lines), axis), 0, {})  120 us
    dot_general x16, matrix products, advance(): acc_im = jnp.dot(lower, w_im, precision=HIGHEST)  47.9 us
    dot_general x16, matrix products, advance(): acc_re = jnp.dot(lower, w_re, precision=HIGHEST)  32.6 us
    all_to_all x1, waiting for transfers between devices, gather_by_exchange(): return lax.all_to_all(copies, axis, dim, dim, tiled=True)  22.5 us
    slice x32, local copies, waits for them, and re-layouts, advance(): ends = (cum_re[-1], cum_im[-1], full_re[-1], full_im[-1])  18.5 us
    dot_general x16, matrix products, advance(): in_re = jnp.dot(grouped, push_re, precision=HIGHEST)  15.3 us
    dot_general x16, matrix products, advance(): in_im = jnp.dot(grouped, push_im, precision=HIGHEST)  15.3 us
    dot_general x16, matrix products, advance(): elapsed = jnp.dot(lower, time_part, precision=HIGHEST)[:, None]  13.1 us
  transfers between devices with their start and end apart: 1, of which 1 were waited for; matrix products, arithmetic and copies ran while one was open for 1% of the time, Pallas kernels for 0%

profile of v1, /device:TPU:33, one launch (start us, length us, event | category | flops | bytes accessed | tf_op | source)
XLA Modules:
  0.0 362.5 jit_solution(3971909153354711741)
XLA Ops:
  0.0 1.7 fusion.44
  1.7 1.5 fusion.46
  3.2 2.3 pad_maximum_fusion
  5.5 5.3 %all-to-all-start = ((bf16[4,256,2048]{2,1,0:T(8,128)(2,1)}), bf16[4,256,2048]{2,1,0:T(8,128)(2,1)}, u32[]{:S(2)}, u32[]{:S(2)}) async-start(bf16[4,256,2048]{2,1,0:T(8,128)(2,1)} %bitcast.149), calls=%async_computation | async-start | bytes 8388608 | tf_op jit(solution)/shard_map/all_to_all | solution.py:13
  15.6 22.5 %all-to-all-done = bf16[4,256,2048]{2,1,0:T(8,128)(2,1)} async-done(((bf16[4,256,2048]{2,1,0:T(8,128)(2,1)}), bf16[4,256,2048]{2,1,0:T(8,128)(2,1)}, u32[]{:S(2)}, u32[]{:S(2)}) %all-to-all-start) | async-done | bytes 4194336 | tf_op jit(solution)/shard_map/all_to_all | solution.py:13
  38.1 4.3 %convolution_convert_fusion.1 = bf16[1024,128]{1,0:T(8,128)(2,1)} fusion(bf16[1024,2048]{1,0:T(8,128)(2,1)} %bitcast.1, bf16[2048,128]{1,0:T(8,128)(2,1)} %param.17), kind=kOutput, calls=%fused_computation.82 | convolution fusion | flops 537001984 | bytes 4980736 | tf_op jit(solution)/shard_map/dot_general | solution.py:131
  43.5 173.4 %while.48 = (s32[]{:T(128)}, f32[512]{0:T(512)S(1)}, f32[512]{0:T(512)S(1)}, f32[512]{0:T(512)}, f32[512]{0:T(512)}, /*index=5*/f32[16,64,512]{2,1,0:T(8,128)}, ...) while((s32[]{:T(128)}, f32[512]{0:T(512)S(1)}, ...), condition=%wide.wide.region_2.3_spmd.clone.clone.clone, body=%wide.wide.region_1.2_spmd.clone.clone.clone.sunk | while | flops 153889792 | bytes 4405837 | solution.py:148
  45.0 1.0 fusion.104
  47.5 2.0 convolution_bitcast_fusion.8
  49.6 3.0 add_dynamic-update-slice_fusion.3
  54.7 1.0 fusion.103
  55.8 1.0 fusion.104
  58.3 2.0 convolution_bitcast_fusion.8
  60.4 3.0 add_dynamic-update-slice_fusion.3
  65.5 1.0 fusion.103
  66.6 1.0 fusion.104
  69.1 2.0 convolution_bitcast_fusion.8
  71.2 3.0 add_dynamic-update-slice_fusion.3
  80.0 2.0 convolution_bitcast_fusion.8
  82.1 3.0 add_dynamic-update-slice_fusion.3
  88.3 1.0 fusion.104
  90.8 2.0 convolution_bitcast_fusion.8
  92.9 3.0 add_dynamic-update-slice_fusion.3
  101.6 2.0 convolution_bitcast_fusion.8
  103.7 3.0 add_dynamic-update-slice_fusion.3
  108.9 1.0 fusion.103
  110.0 1.0 fusion.104
  112.5 2.0 convolution_bitcast_fusion.8
  114.6 3.0 add_dynamic-update-slice_fusion.3
  119.7 1.0 fusion.103
  123.3 2.0 convolution_bitcast_fusion.8
  125.4 3.0 add_dynamic-update-slice_fusion.3
  134.1 2.0 convolution_bitcast_fusion.8
  136.2 3.0 add_dynamic-update-slice_fusion.3
  144.9 2.0 convolution_bitcast_fusion.8
  147.1 3.0 add_dynamic-update-slice_fusion.3
  155.8 2.0 convolution_bitcast_fusion.8
  157.9 3.0 add_dynamic-update-slice_fusion.3
  163.0 1.0 fusion.103
  164.1 1.0 fusion.104
  166.6 2.0 convolution_bitcast_fusion.8
  168.8 3.0 add_dynamic-update-slice_fusion.3
  173.9 1.0 fusion.103
  175.0 1.0 fusion.104
  177.5 2.0 convolution_bitcast_fusion.8
  179.6 3.0 add_dynamic-update-slice_fusion.3
  184.7 1.0 fusion.103
  185.8 1.0 fusion.104
  188.3 2.0 convolution_bitcast_fusion.8
  190.4 3.0 add_dynamic-update-slice_fusion.3
  196.7 1.0 fusion.104
  199.2 2.0 convolution_bitcast_fusion.8
  201.3 3.0 add_dynamic-update-slice_fusion.3
  206.4 1.0 fusion.103
  207.5 1.0 fusion.104
  210.0 2.0 convolution_bitcast_fusion.8
  212.1 3.0 add_dynamic-update-slice_fusion.3
  217.6 120.1 %all-gather.1 = f32[64,4,512]{2,1,0:T(4,128)S(1)} all-gather(f32[1,4,512]{2,1,0:T(4,128)S(1)} %maximum_bitcast_fusion), channel_id=2, replica_groups=mesh['grp'=2,'sp'=64,'tp'=4] {'sp'}, dimensions={0}, use_global_device_ids=true | all-gather | bytes 532480 | tf_op jit(solution)/shard_map/all_gather | solution.py:24
  338.1 5.1 %while.47 = (s32[]{:T(128)}, f32[512]{0:T(512)S(1)}, f32[512]{0:T(512)S(1)}, s32[]{:T(128)}, f32[64,512]{1,0:T(8,128)S(1)}, /*index=5*/f32[64,512]{1,0:T(8,128)S...) while((s32[]{:T(128)}, f32[512]{0:T(512)S(1)}, f32[512]{0:T(512)S(1)}, ...), condition=%wide.region_4.5_spmd.clone, body=%wide.region_3.4_spmd.clone.sunk | while | flops 6148 | bytes 32897 | solution.py:44
  343.3 4.6 %multiply_add_fusion.5 = (f32[16,64,512]{2,1,0:T(8,128)S(1)}, f32[16,64,512]{2,1,0:T(8,128)S(1)}) fusion(f32[16,64,512]{2,1,0:T(8,128)} %get-tuple-element.435, f32[16,64,512]{2,1,0:T(8,128)} %get-tuple-element.437, f32[16,64,512]{2,1,0:T(8,128)} %get-tuple-element.429, f32[512]{0:T(512)S(1)} %get-tuple-element.436, f32[512]{0:T(512)S(1)} %get-tuple-element.434, ...), kind=kLoop, calls=%fused_computation.79 | loop fusion | flops 4194304 | bytes 12587008 | tf_op jit(solution)/shard_map/add | solution.py:161
  347.9 1.8 fusion.59
  349.7 1.8 fusion.54
  351.7 8.9 %all_to_all.25 = bf16[4,256,128]{1,2,0:T(8,128)(2,1)S(1)} all-to-all(bf16[4,256,128]{1,2,0:T(8,128)(2,1)S(1)} %copy.20), channel_id=1, replica_groups=mesh['grp'=2,'sp'=64,'tp'=4] {'tp'}, dimensions={0} | all-to-all | bytes 524288 | tf_op jit(solution)/shard_map/all_to_all | solution.py:163
  360.8 1.7 convolution_convert_fusion
  (595 shorter events, 82.9 us)
Async XLA Ops:
  0.0 360.8 %copy-start = (bf16[512,2048]{1,0:T(8,128)(2,1)S(1)}, bf16[512,2048]{1,0:T(8,128)(2,1)}, u32[]{:S(2)}) copy-start(bf16[512,2048]{1,0:T(8,128)(2,1)} %param.23) | copy-start | bytes 6291460
  5.5 7.3 %copy-start.12 = (f32[1024]{0:T(1024)S(1)}, f32[1024]{0:T(1024)}, u32[]{:S(2)}) copy-start(f32[1024]{0:T(1024)} %param.15) | copy-start | bytes 12292
  5.5 8.0 %copy-start.3 = (f32[2,8,16,64]{3,2,1,0:T(8,128)S(1)}, f32[2,8,16,64]{3,2,1,0:T(8,128)}, u32[]{:S(2)}) copy-start(f32[2,8,16,64]{3,2,1,0:T(8,128)} %param.21) | copy-start | bytes 196612
  5.5 32.6 %all-to-all-start = ((bf16[4,256,2048]{2,1,0:T(8,128)(2,1)}), bf16[4,256,2048]{2,1,0:T(8,128)(2,1)}, u32[]{:S(2)}, u32[]{:S(2)}) async-start(bf16[4,256,2048]{2,1,0:T(8,128)(2,1)} %bitcast.149), calls=%async_computation | async-start | bytes 8388608 | tf_op jit(solution)/shard_map/all_to_all | solution.py:13
  54.6 5.7 %copy-start.5 = (f32[1,512]{1,0:T(1,128)S(1)}, f32[1,512]{1,0:T(1,128)}, u32[]{:S(2)}) copy-start(f32[1,512]{1,0:T(1,128)} %get-tuple-element.1028) | copy-start | bytes 6148 | tf_op jit(solution)/shard_map/while
  54.7 5.7 %copy-start.10 = (f32[512]{0:T(512)S(1)}, f32[512]{0:T(512)}, u32[]{:S(2)}) copy-start(f32[512]{0:T(512)} %get-tuple-element.1001) | copy-start | bytes 6148 | tf_op jit(solution)/shard_map/while
  54.7 5.7 %copy-start.11 = (f32[512]{0:T(512)S(1)}, f32[512]{0:T(512)}, u32[]{:S(2)}) copy-start(f32[512]{0:T(512)} %get-tuple-element.1002) | copy-start | bytes 6148 | tf_op jit(solution)/shard_map/while
  54.7 5.7 %copy-start.14 = (f32[512]{0:T(512)S(1)}, f32[512]{0:T(512)}, u32[]{:S(2)}) copy-start(f32[512]{0:T(512)} %get-tuple-element.1038) | copy-start | bytes 6148 | tf_op jit(solution)/shard_map/while
  54.7 5.7 %copy-start.15 = (f32[1,512]{1,0:T(1,128)S(1)}, f32[1,512]{1,0:T(1,128)}, u32[]{:S(2)}) copy-start(f32[1,512]{1,0:T(1,128)} %get-tuple-element.1032) | copy-start | bytes 6148 | tf_op jit(solution)/shard_map/while
  65.5 5.7 %copy-start.5 = (f32[1,512]{1,0:T(1,128)S(1)}, f32[1,512]{1,0:T(1,128)}, u32[]{:S(2)}) copy-start(f32[1,512]{1,0:T(1,128)} %get-tuple-element.1028) | copy-start | bytes 6148 | tf_op jit(solution)/shard_map/while
  65.5 5.7 %copy-start.10 = (f32[512]{0:T(512)S(1)}, f32[512]{0:T(512)}, u32[]{:S(2)}) copy-start(f32[512]{0:T(512)} %get-tuple-element.1001) | copy-start | bytes 6148 | tf_op jit(solution)/shard_map/while
  108.8 5.7 %copy-start.5 = (f32[1,512]{1,0:T(1,128)S(1)}, f32[1,512]{1,0:T(1,128)}, u32[]{:S(2)}) copy-start(f32[1,512]{1,0:T(1,128)} %get-tuple-element.1028) | copy-start | bytes 6148 | tf_op jit(solution)/shard_map/while
  108.8 5.7 %copy-start.10 = (f32[512]{0:T(512)S(1)}, f32[512]{0:T(512)}, u32[]{:S(2)}) copy-start(f32[512]{0:T(512)} %get-tuple-element.1001) | copy-start | bytes 6148 | tf_op jit(solution)/shard_map/while
  108.8 5.7 %copy-start.11 = (f32[512]{0:T(512)S(1)}, f32[512]{0:T(512)}, u32[]{:S(2)}) copy-start(f32[512]{0:T(512)} %get-tuple-element.1002) | copy-start | bytes 6148 | tf_op jit(solution)/shard_map/while
  108.8 5.7 %copy-start.14 = (f32[512]{0:T(512)S(1)}, f32[512]{0:T(512)}, u32[]{:S(2)}) copy-start(f32[512]{0:T(512)} %get-tuple-element.1038) | copy-start | bytes 6148 | tf_op jit(solution)/shard_map/while
  108.8 5.7 %copy-start.15 = (f32[1,512]{1,0:T(1,128)S(1)}, f32[1,512]{1,0:T(1,128)}, u32[]{:S(2)}) copy-start(f32[1,512]{1,0:T(1,128)} %get-tuple-element.1032) | copy-start | bytes 6148 | tf_op jit(solution)/shard_map/while
  119.6 5.7 %copy-start.5 = (f32[1,512]{1,0:T(1,128)S(1)}, f32[1,512]{1,0:T(1,128)}, u32[]{:S(2)}) copy-start(f32[1,512]{1,0:T(1,128)} %get-tuple-element.1028) | copy-start | bytes 6148 | tf_op jit(solution)/shard_map/while
  119.6 5.7 %copy-start.10 = (f32[512]{0:T(512)S(1)}, f32[512]{0:T(512)}, u32[]{:S(2)}) copy-start(f32[512]{0:T(512)} %get-tuple-element.1001) | copy-start | bytes 6148 | tf_op jit(solution)/shard_map/while
  119.7 5.7 %copy-start.11 = (f32[512]{0:T(512)S(1)}, f32[512]{0:T(512)}, u32[]{:S(2)}) copy-start(f32[512]{0:T(512)} %get-tuple-element.1002) | copy-start | bytes 6148 | tf_op jit(solution)/shard_map/while
  119.7 5.7 %copy-start.14 = (f32[512]{0:T(512)S(1)}, f32[512]{0:T(512)}, u32[]{:S(2)}) copy-start(f32[512]{0:T(512)} %get-tuple-element.1038) | copy-start | bytes 6148 | tf_op jit(solution)/shard_map/while
  119.7 5.7 %copy-start.15 = (f32[1,512]{1,0:T(1,128)S(1)}, f32[1,512]{1,0:T(1,128)}, u32[]{:S(2)}) copy-start(f32[1,512]{1,0:T(1,128)} %get-tuple-element.1032) | copy-start | bytes 6148 | tf_op jit(solution)/shard_map/while
  130.5 5.7 %copy-start.5 = (f32[1,512]{1,0:T(1,128)S(1)}, f32[1,512]{1,0:T(1,128)}, u32[]{:S(2)}) copy-start(f32[1,512]{1,0:T(1,128)} %get-tuple-element.1028) | copy-start | bytes 6148 | tf_op jit(solution)/shard_map/while
  130.5 5.7 %copy-start.10 = (f32[512]{0:T(512)S(1)}, f32[512]{0:T(512)}, u32[]{:S(2)}) copy-start(f32[512]{0:T(512)} %get-tuple-element.1001) | copy-start | bytes 6148 | tf_op jit(solution)/shard_map/while
  130.5 5.7 %copy-start.11 = (f32[512]{0:T(512)S(1)}, f32[512]{0:T(512)}, u32[]{:S(2)}) copy-start(f32[512]{0:T(512)} %get-tuple-element.1002) | copy-start | bytes 6148 | tf_op jit(solution)/shard_map/while
  130.5 5.7 %copy-start.14 = (f32[512]{0:T(512)S(1)}, f32[512]{0:T(512)}, u32[]{:S(2)}) copy-start(f32[512]{0:T(512)} %get-tuple-element.1038) | copy-start | bytes 6148 | tf_op jit(solution)/shard_map/while
  130.5 5.7 %copy-start.15 = (f32[1,512]{1,0:T(1,128)S(1)}, f32[1,512]{1,0:T(1,128)}, u32[]{:S(2)}) copy-start(f32[1,512]{1,0:T(1,128)} %get-tuple-element.1032) | copy-start | bytes 6148 | tf_op jit(solution)/shard_map/while
  141.3 5.7 %copy-start.5 = (f32[1,512]{1,0:T(1,128)S(1)}, f32[1,512]{1,0:T(1,128)}, u32[]{:S(2)}) copy-start(f32[1,512]{1,0:T(1,128)} %get-tuple-element.1028) | copy-start | bytes 6148 | tf_op jit(solution)/shard_map/while
  141.3 5.7 %copy-start.10 = (f32[512]{0:T(512)S(1)}, f32[512]{0:T(512)}, u32[]{:S(2)}) copy-start(f32[512]{0:T(512)} %get-tuple-element.1001) | copy-start | bytes 6148 | tf_op jit(solution)/shard_map/while
  141.3 5.7 %copy-start.11 = (f32[512]{0:T(512)S(1)}, f32[512]{0:T(512)}, u32[]{:S(2)}) copy-start(f32[512]{0:T(512)} %get-tuple-element.1002) | copy-start | bytes 6148 | tf_op jit(solution)/shard_map/while
  141.3 5.7 %copy-start.14 = (f32[512]{0:T(512)S(1)}, f32[512]{0:T(512)}, u32[]{:S(2)}) copy-start(f32[512]{0:T(512)} %get-tuple-element.1038) | copy-start | bytes 6148 | tf_op jit(solution)/shard_map/while
  141.3 5.7 %copy-start.15 = (f32[1,512]{1,0:T(1,128)S(1)}, f32[1,512]{1,0:T(1,128)}, u32[]{:S(2)}) copy-start(f32[1,512]{1,0:T(1,128)} %get-tuple-element.1032) | copy-start | bytes 6148 | tf_op jit(solution)/shard_map/while
  152.1 5.7 %copy-start.5 = (f32[1,512]{1,0:T(1,128)S(1)}, f32[1,512]{1,0:T(1,128)}, u32[]{:S(2)}) copy-start(f32[1,512]{1,0:T(1,128)} %get-tuple-element.1028) | copy-start | bytes 6148 | tf_op jit(solution)/shard_map/while
  152.1 5.7 %copy-start.10 = (f32[512]{0:T(512)S(1)}, f32[512]{0:T(512)}, u32[]{:S(2)}) copy-start(f32[512]{0:T(512)} %get-tuple-element.1001) | copy-start | bytes 6148 | tf_op jit(solution)/shard_map/while
  152.2 5.7 %copy-start.11 = (f32[512]{0:T(512)S(1)}, f32[512]{0:T(512)}, u32[]{:S(2)}) copy-start(f32[512]{0:T(512)} %get-tuple-element.1002) | copy-start | bytes 6148 | tf_op jit(solution)/shard_map/while
  152.2 5.7 %copy-start.14 = (f32[512]{0:T(512)S(1)}, f32[512]{0:T(512)}, u32[]{:S(2)}) copy-start(f32[512]{0:T(512)} %get-tuple-element.1038) | copy-start | bytes 6148 | tf_op jit(solution)/shard_map/while
  152.2 5.7 %copy-start.15 = (f32[1,512]{1,0:T(1,128)S(1)}, f32[1,512]{1,0:T(1,128)}, u32[]{:S(2)}) copy-start(f32[1,512]{1,0:T(1,128)} %get-tuple-element.1032) | copy-start | bytes 6148 | tf_op jit(solution)/shard_map/while
  163.0 5.7 %copy-start.5 = (f32[1,512]{1,0:T(1,128)S(1)}, f32[1,512]{1,0:T(1,128)}, u32[]{:S(2)}) copy-start(f32[1,512]{1,0:T(1,128)} %get-tuple-element.1028) | copy-start | bytes 6148 | tf_op jit(solution)/shard_map/while
  163.0 5.7 %copy-start.10 = (f32[512]{0:T(512)S(1)}, f32[512]{0:T(512)}, u32[]{:S(2)}) copy-start(f32[512]{0:T(512)} %get-tuple-element.1001) | copy-start | bytes 6148 | tf_op jit(solution)/shard_map/while
  163.0 5.7 %copy-start.11 = (f32[512]{0:T(512)S(1)}, f32[512]{0:T(512)}, u32[]{:S(2)}) copy-start(f32[512]{0:T(512)} %get-tuple-element.1002) | copy-start | bytes 6148 | tf_op jit(solution)/shard_map/while
  163.0 5.7 %copy-start.14 = (f32[512]{0:T(512)S(1)}, f32[512]{0:T(512)}, u32[]{:S(2)}) copy-start(f32[512]{0:T(512)} %get-tuple-element.1038) | copy-start | bytes 6148 | tf_op jit(solution)/shard_map/while
  163.0 5.7 %copy-start.15 = (f32[1,512]{1,0:T(1,128)S(1)}, f32[1,512]{1,0:T(1,128)}, u32[]{:S(2)}) copy-start(f32[1,512]{1,0:T(1,128)} %get-tuple-element.1032) | copy-start | bytes 6148 | tf_op jit(solution)/shard_map/while
  173.8 5.7 %copy-start.5 = (f32[1,512]{1,0:T(1,128)S(1)}, f32[1,512]{1,0:T(1,128)}, u32[]{:S(2)}) copy-start(f32[1,512]{1,0:T(1,128)} %get-tuple-element.1028) | copy-start | bytes 6148 | tf_op jit(solution)/shard_map/while
  173.8 5.7 %copy-start.10 = (f32[512]{0:T(512)S(1)}, f32[512]{0:T(512)}, u32[]{:S(2)}) copy-start(f32[512]{0:T(512)} %get-tuple-element.1001) | copy-start | bytes 6148 | tf_op jit(solution)/shard_map/while
  173.9 5.7 %copy-start.11 = (f32[512]{0:T(512)S(1)}, f32[512]{0:T(512)}, u32[]{:S(2)}) copy-start(f32[512]{0:T(512)} %get-tuple-element.1002) | copy-start | bytes 6148 | tf_op jit(solution)/shard_map/while
  173.9 5.7 %copy-start.14 = (f32[512]{0:T(512)S(1)}, f32[512]{0:T(512)}, u32[]{:S(2)}) copy-start(f32[512]{0:T(512)} %get-tuple-element.1038) | copy-start | bytes 6148 | tf_op jit(solution)/shard_map/while
  173.9 5.7 %copy-start.15 = (f32[1,512]{1,0:T(1,128)S(1)}, f32[1,512]{1,0:T(1,128)}, u32[]{:S(2)}) copy-start(f32[1,512]{1,0:T(1,128)} %get-tuple-element.1032) | copy-start | bytes 6148 | tf_op jit(solution)/shard_map/while
  184.7 5.7 %copy-start.5 = (f32[1,512]{1,0:T(1,128)S(1)}, f32[1,512]{1,0:T(1,128)}, u32[]{:S(2)}) copy-start(f32[1,512]{1,0:T(1,128)} %get-tuple-element.1028) | copy-start | bytes 6148 | tf_op jit(solution)/shard_map/while
  184.7 5.7 %copy-start.10 = (f32[512]{0:T(512)S(1)}, f32[512]{0:T(512)}, u32[]{:S(2)}) copy-start(f32[512]{0:T(512)} %get-tuple-element.1001) | copy-start | bytes 6148 | tf_op jit(solution)/shard_map/while
  184.7 5.7 %copy-start.11 = (f32[512]{0:T(512)S(1)}, f32[512]{0:T(512)}, u32[]{:S(2)}) copy-start(f32[512]{0:T(512)} %get-tuple-element.1002) | copy-start | bytes 6148 | tf_op jit(solution)/shard_map/while
  184.7 5.7 %copy-start.14 = (f32[512]{0:T(512)S(1)}, f32[512]{0:T(512)}, u32[]{:S(2)}) copy-start(f32[512]{0:T(512)} %get-tuple-element.1038) | copy-start | bytes 6148 | tf_op jit(solution)/shard_map/while
  184.7 5.7 %copy-start.15 = (f32[1,512]{1,0:T(1,128)S(1)}, f32[1,512]{1,0:T(1,128)}, u32[]{:S(2)}) copy-start(f32[1,512]{1,0:T(1,128)} %get-tuple-element.1032) | copy-start | bytes 6148 | tf_op jit(solution)/shard_map/while
  195.5 5.7 %copy-start.5 = (f32[1,512]{1,0:T(1,128)S(1)}, f32[1,512]{1,0:T(1,128)}, u32[]{:S(2)}) copy-start(f32[1,512]{1,0:T(1,128)} %get-tuple-element.1028) | copy-start | bytes 6148 | tf_op jit(solution)/shard_map/while
  195.5 5.7 %copy-start.10 = (f32[512]{0:T(512)S(1)}, f32[512]{0:T(512)}, u32[]{:S(2)}) copy-start(f32[512]{0:T(512)} %get-tuple-element.1001) | copy-start | bytes 6148 | tf_op jit(solution)/shard_map/while
  195.5 5.7 %copy-start.11 = (f32[512]{0:T(512)S(1)}, f32[512]{0:T(512)}, u32[]{:S(2)}) copy-start(f32[512]{0:T(512)} %get-tuple-element.1002) | copy-start | bytes 6148 | tf_op jit(solution)/shard_map/while
  195.5 5.7 %copy-start.14 = (f32[512]{0:T(512)S(1)}, f32[512]{0:T(512)}, u32[]{:S(2)}) copy-start(f32[512]{0:T(512)} %get-tuple-element.1038) | copy-start | bytes 6148 | tf_op jit(solution)/shard_map/while
  195.5 5.7 %copy-start.15 = (f32[1,512]{1,0:T(1,128)S(1)}, f32[1,512]{1,0:T(1,128)}, u32[]{:S(2)}) copy-start(f32[1,512]{1,0:T(1,128)} %get-tuple-element.1032) | copy-start | bytes 6148 | tf_op jit(solution)/shard_map/while
  206.3 5.7 %copy-start.5 = (f32[1,512]{1,0:T(1,128)S(1)}, f32[1,512]{1,0:T(1,128)}, u32[]{:S(2)}) copy-start(f32[1,512]{1,0:T(1,128)} %get-tuple-element.1028) | copy-start | bytes 6148 | tf_op jit(solution)/shard_map/while
  206.4 5.7 %copy-start.10 = (f32[512]{0:T(512)S(1)}, f32[512]{0:T(512)}, u32[]{:S(2)}) copy-start(f32[512]{0:T(512)} %get-tuple-element.1001) | copy-start | bytes 6148 | tf_op jit(solution)/shard_map/while
  206.4 5.7 %copy-start.11 = (f32[512]{0:T(512)S(1)}, f32[512]{0:T(512)}, u32[]{:S(2)}) copy-start(f32[512]{0:T(512)} %get-tuple-element.1002) | copy-start | bytes 6148 | tf_op jit(solution)/shard_map/while
  206.4 5.7 %copy-start.14 = (f32[512]{0:T(512)S(1)}, f32[512]{0:T(512)}, u32[]{:S(2)}) copy-start(f32[512]{0:T(512)} %get-tuple-element.1038) | copy-start | bytes 6148 | tf_op jit(solution)/shard_map/while
  206.4 5.7 %copy-start.15 = (f32[1,512]{1,0:T(1,128)S(1)}, f32[1,512]{1,0:T(1,128)}, u32[]{:S(2)}) copy-start(f32[1,512]{1,0:T(1,128)} %get-tuple-element.1032) | copy-start | bytes 6148 | tf_op jit(solution)/shard_map/while
  216.9 121.2 %copy-start.6 = (f32[512]{0:T(512)S(1)}, f32[512]{0:T(512)}, u32[]{:S(2)}) copy-start(f32[512]{0:T(512)} %custom-call) | copy-start | bytes 6148
  216.9 121.2 %copy-start.7 = (f32[512]{0:T(512)S(1)}, f32[512]{0:T(512)}, u32[]{:S(2)}) copy-start(f32[512]{0:T(512)} %custom-call.1) | copy-start | bytes 6148
  349.7 11.0 %copy-start.13 = (f32[512]{0:T(512)S(1)}, f32[512]{0:T(512)}, u32[]{:S(2)}) copy-start(f32[512]{0:T(512)} %param.22) | copy-start | bytes 6148
  (28 other events, 153.5 us)
